TPU v7x, 512 devices: a 4x2x32 block of a 4x8x32 slice. The times are simulated.
512 devices in a mesh: grp: 2 (over y), sp: 32 (over z), tp: 8 (over x, core).
Axes of the slice: x: 4, y: 2, z: 32, core: 2. Of those that a mesh axis runs over, the one named last changes fastest.
The devices are a block of a 4x8x32 slice.
Arguments:
- starting_stream: bfloat16 [24576, 2048], P(('grp', 'sp'), 'tp'), parts along dimension 0, may hold values from -45 to 45
- multiplier_matrix: bfloat16 [2, 2048, 2048], P(None, 'sp', 'tp'), may hold values from -0.125 to 0.125
- memory_path_matrix: bfloat16 [2, 2048, 2048], P(None, 'sp', 'tp'), may hold values from -0.125 to 0.125
- filter_coefficients: bfloat16 [2, 4, 2048], P(None, None, 'tp'), may hold values from -3 to 3
- memory_valve_matrix: bfloat16 [2, 8, 256, 256], P(None, 'tp'), may hold values from -0.375 to 0.375
- entry_valve_matrix: bfloat16 [2, 8, 256, 256], P(None, 'tp'), may hold values from -0.375 to 0.375
- forgetting_parameters: float32 [2, 2048], P(None, 'tp'), may hold values from 3 to 15
- timestep_forgetting_multiplier: float32 [24576], P(('grp', 'sp')), parts along dimension 0, may hold values from 0.5 to 2
- spike_extra: float32 [24576, 2048], P(('grp', 'sp'), 'tp'), parts along dimension 0, may hold values from -0.7 to 0
- exit_projector_matrix: bfloat16 [2, 2048, 2048], P(None, 'tp', 'sp'), may hold values from -0.125 to 0.125
- prelude_rms_gains: float32 [2, 2048], replicated, may hold values from 0.1 to 1.9
- finishing_rms_gains: float32 [2048], P('tp'), may hold values from 0.1 to 1.9
Outputs:
- result: bfloat16 [24576, 2048], P(('grp', 'sp'), 'tp'), parts along dimension 0
There are 2 independent parts, one for each index of `grp`. A program takes and returns all parts, laid end to end along the dimension named above; an argument that names none is the same for every part. Nothing has to cross between parts.
All inputs are finite; a program needn't handle non-finite values.
Results may differ from a plain program's by a relative error of at most 0.015.
Values may be sent and summed in bfloat16 or wider, within the bound.
A program may use at most 64 MiB of HBM per device.

v0:
```python
import jax
import jax.numpy as jnp
from jax import lax
from jax.sharding import PartitionSpec as P

BLOCK_W = 256
EPSILON = 1e-06
SQUASH_POWER = 8.0


def sent_to_all(x, axis):
    copies = jnp.broadcast_to(x, (lax.axis_size(axis), *x.shape))
    return lax.all_to_all(copies, axis, split_axis=0, concat_axis=0, tiled=True)


def laid_out(tiles, dim):
    lengths = list(tiles.shape[1:])
    lengths[dim] *= tiles.shape[0]
    return jnp.moveaxis(tiles, 0, dim).reshape(lengths)


def gather_directly(x, axis, dim):
    tiles = sent_to_all(x, axis)
    return laid_out(tiles, dim)


def in_one_piece(arrays, axis, dim, along):
    widths = [a.shape[along] for a in arrays]
    both = jnp.concatenate(arrays, axis=along)
    whole = lax.all_gather(both, axis, axis=dim, tiled=True)
    return tuple(jnp.split(whole, [sum(widths[:k]) for k in range(1, len(widths))], axis=along))


def from_behind(value, axis, steps):
    count = lax.axis_size(axis)
    first, last = (max(0, -steps), min(count, count - steps))
    return lax.ppermute(value, axis, [(source, source + steps) for source in range(first, last)])


def gathered_once(x, axis):
    leaves = jax.tree.leaves(x)
    turns = sorted(range(len(leaves)), key=lambda k: -leaves[k].size)
    width = (1, *leaves[turns[0]].shape)[-1]
    lines = [
        jnp.pad(leaves[k].reshape(-1), (0, -leaves[k].size % width)).reshape(-1, width)
        for k in turns
    ]
    both, at, found = (lax.all_gather(jnp.concatenate(lines), axis), 0, {})
    for k, line in zip(turns, lines):
        slab = both[:, at : at + len(line)].reshape(len(both), -1)
        found[k] = slab[:, : leaves[k].size].reshape(-1, *leaves[k].shape)
        at += len(line)
    numbers = iter(range(len(leaves)))
    return jax.tree.map(lambda _: found[next(numbers)], x)


def carried_in(part, axis, combine, identity):
    place = lax.axis_index(axis)
    gathered = gathered_once(part, axis)
    state = jax.tree.map(lambda a, e: jnp.zeros_like(a) + jnp.asarray(e, a.dtype), part, identity)

    def one(lap, state):
        return combine(
            state, jax.tree.map(lambda a: lax.dynamic_index_in_dim(a, lap, 0, False), gathered)
        )

    return lax.fori_loop(0, place, one, state)


def split_up(x, dim, count):
    before, after = (x.shape[:dim], x.shape[dim + 1 :])
    return jnp.moveaxis(x.reshape(*before, count, -1, *after), dim, 0)


def summed_on_arrival(x, axis, dim):
    tiles = split_up(x, dim, lax.axis_size(axis))
    arrived = lax.all_to_all(tiles, axis, split_axis=0, concat_axis=0, tiled=True)
    return arrived.astype(jnp.float32).sum(axis=0)


def of_everyone(x, axis):
    everything = sent_to_all(x, axis)
    return jnp.sum(everything, axis=0)


def combine_pairs(earlier, later):
    return (earlier[0] * later[0], later[0] * earlier[1] + later[1])


def gather_rows(own_cols):
    return gather_directly(own_cols, "tp", 1)


def fetch_layer(multiplier_matrix, memory_path_matrix, exit_projector_matrix, tier_number):
    in_pair = in_one_piece(
        (multiplier_matrix[tier_number], memory_path_matrix[tier_number]), "sp", 0, 1
    )
    out_full = lax.all_gather(exit_projector_matrix[tier_number], "sp", axis=1, tiled=True)
    return (in_pair[0], in_pair[1], out_full)


def on_device(
    starting_stream,
    multiplier_matrix,
    memory_path_matrix,
    filter_coefficients,
    memory_valve_matrix,
    entry_valve_matrix,
    forgetting_parameters,
    timestep_forgetting_multiplier,
    spike_extra,
    exit_projector_matrix,
    prelude_rms_gains,
    finishing_rms_gains,
):
    tok_rows = starting_stream.shape[0]
    channels = memory_path_matrix.shape[2]
    own_cols = starting_stream
    full_rows = gather_rows(starting_stream)
    fetched = fetch_layer(multiplier_matrix, memory_path_matrix, exit_projector_matrix, 0)
    for tier_number in range(memory_path_matrix.shape[0]):
        floats = full_rows.astype(jnp.float32)
        mean_square = jnp.mean(floats * floats, axis=1, keepdims=True)
        normed = (
            floats * lax.rsqrt(mean_square + EPSILON) * prelude_rms_gains[tier_number][None, :]
        ).astype(jnp.bfloat16)
        branch_acc = jnp.dot(normed, fetched[0], preferred_element_type=jnp.float32)
        recur_acc = jnp.dot(normed, fetched[1], preferred_element_type=jnp.float32)
        out_full = fetched[2]
        if tier_number + 1 < memory_path_matrix.shape[0]:
            fetched = fetch_layer(
                multiplier_matrix, memory_path_matrix, exit_projector_matrix, tier_number + 1
            )
        branch = branch_acc.astype(jnp.bfloat16)
        recurrent = recur_acc.astype(jnp.bfloat16)
        taps_now = filter_coefficients[tier_number]
        reach_back = taps_now.shape[0] - 1
        halo_rows = from_behind(recurrent[tok_rows - reach_back :], "sp", 1)
        extended = jnp.concatenate([halo_rows, recurrent], axis=0)
        conv_sum = jnp.zeros((tok_rows, channels), jnp.float32)
        for offset in range(taps_now.shape[0]):
            conv_sum = conv_sum + extended[offset : offset + tok_rows].astype(
                jnp.float32
            ) * taps_now[offset].astype(jnp.float32)
        convolved = conv_sum.astype(jnp.bfloat16)
        blocks = convolved.reshape(tok_rows, channels // BLOCK_W, BLOCK_W)
        reset_gate = jax.nn.sigmoid(
            jnp.einsum(
                "tnc,ncd->tnd",
                blocks,
                memory_valve_matrix[tier_number],
                preferred_element_type=jnp.float32,
            ).reshape(tok_rows, channels)
        )
        inject = jax.nn.sigmoid(
            jnp.einsum(
                "tnc,ncd->tnd",
                blocks,
                entry_valve_matrix[tier_number],
                preferred_element_type=jnp.float32,
            ).reshape(tok_rows, channels)
        )
        logarithmic_persistence = (
            -SQUASH_POWER
            * reset_gate
            * jax.nn.softplus(-forgetting_parameters[tier_number])[None, :]
            * timestep_forgetting_multiplier[:, None]
            + spike_extra
        )
        keep_rate = jnp.exp(logarithmic_persistence)
        driven = (
            inject
            * convolved.astype(jnp.float32)
            * jnp.sqrt(-jnp.expm1(2.0 * logarithmic_persistence))
        )
        keep_cum, state_local = lax.associative_scan(combine_pairs, (keep_rate, driven), axis=0)
        identity = (jnp.ones((channels,), jnp.float32), jnp.zeros((channels,), jnp.float32))
        carried = carried_in((keep_cum[-1], state_local[-1]), "sp", combine_pairs, identity)
        state_seq = state_local + keep_cum * carried[1][None, :]
        mixed_in = (jax.nn.gelu(branch.astype(jnp.float32)) * state_seq).astype(jnp.bfloat16)
        partial_value = jnp.dot(mixed_in, out_full, preferred_element_type=jnp.float32)
        mixed_sum = summed_on_arrival(partial_value.astype(jnp.bfloat16), "tp", 1)
        own_cols = (own_cols.astype(jnp.float32) + mixed_sum).astype(jnp.bfloat16)
        if tier_number + 1 < memory_path_matrix.shape[0]:
            full_rows = gather_rows(own_cols)
    floats = own_cols.astype(jnp.float32)
    full_width = floats.shape[1] * lax.axis_size("tp")
    square_sum = of_everyone(jnp.sum(floats * floats, axis=1), "tp")
    inv_rms = lax.rsqrt(square_sum / full_width + EPSILON)
    return (floats * inv_rms[:, None] * finishing_rms_gains[None, :]).astype(jnp.bfloat16)


def solution(mesh):
    return jax.shard_map(
        on_device,
        mesh=mesh,
        in_specs=(
            P(("grp", "sp"), "tp"),
            P(None, "sp", "tp"),
            P(None, "sp", "tp"),
            P(None, None, "tp"),
            P(None, "tp", None, None),
            P(None, "tp", None, None),
            P(None, "tp"),
            P(("grp", "sp")),
            P(("grp", "sp"), "tp"),
            P(None, "tp", "sp"),
            P(),
            P("tp"),
        ),
        out_specs=P(("grp", "sp"), "tp"),
        check_vma=False,
    )
```

profile of v0, /device:TPU:33, one launch (start us, length us, event | category | flops | bytes accessed | tf_op | source)
XLA Modules:
  0.0 602.2 jit_solution(12787368369105031495)
XLA Ops:
  8.1 1.4 fusion.135
  12.0 45.1 %all-to-all-start = ((bf16[8,384,256]{1,2,0:T(8,128)(2,1)}), bf16[8,384,256]{1,2,0:T(8,128)(2,1)S(1)}, u32[]{:S(2)}, u32[]{:S(2)}) async-start(bf16[8,384,256]{1,2,0:T(8,128)(2,1)} %broadcast_in_dim.6), calls=%async_computation | async-start | bytes 3145728 | tf_op jit(solution)/shard_map/all_to_all | solution.py:13
  59.1 18.7 %all-to-all-done = bf16[8,384,256]{1,2,0:T(8,128)(2,1)S(1)} async-done(((bf16[8,384,256]{1,2,0:T(8,128)(2,1)}), bf16[8,384,256]{1,2,0:T(8,128)(2,1)S(1)}, u32[]{:S(2)}, u32[]{:S(2)}) %all-to-all-start) | async-done | bytes 1572896 | tf_op jit(solution)/shard_map/all_to_all | solution.py:13
  78.6 72.2 %all-gather.11.cloned.1.call-done = bf16[2048,512]{1,0:T(8,128)(2,1)} async-done(((bf16[64,512]{1,0:T(8,128)(2,1)}), bf16[2048,512]{1,0:T(8,128)(2,1)}) %all-gather.11.cloned.1.call-update) | async-done | bytes 2097168 | tf_op jit(solution)/shard_map/all_gather | solution.py:30
  150.8 1.8 convolution_convert_fusion.4
  152.7 1.7 collective-permute-start
  174.2 1.5 pad.227
  177.4 40.9 %all-gather.4 = f32[32,2,256]{2,1,0:T(2,128)S(1)} all-gather(f32[1,2,256]{2,1,0:T(2,128)S(1)} %maximum_bitcast_fusion), channel_id=2, replica_groups=mesh['grp'=2,'sp'=32,'tp'=8] {'sp'}, dimensions={0}, use_global_device_ids=true | all-gather | bytes 67584 | tf_op jit(solution)/shard_map/all_gather | solution.py:48
  218.4 59.8 %all-gather.15.cloned.1.call-done = bf16[1,256,2048]{1,2,0:T(8,128)(2,1)} async-done(((bf16[1,256,64]{1,2,0:T(8,128)(2,1)}), bf16[1,256,2048]{1,2,0:T(8,128)(2,1)}) %all-gather.15.cloned.1.call-update) | async-done | bytes 1048592 | tf_op jit(solution)/shard_map/all_gather | solution.py:98
  278.2 3.8 convolution_convert_fusion.1
  282.1 46.2 %all_to_all.26 = bf16[8,384,256]{2,1,0:T(8,128)(2,1)S(1)} all-to-all(bf16[8,384,256]{2,1,0:T(8,128)(2,1)S(1)} %bitcast.108), channel_id=1, replica_groups=mesh['grp'=2,'sp'=32,'tp'=8] {'tp'}, dimensions={0} | all-to-all | bytes 3145728 | tf_op jit(solution)/shard_map/all_to_all | solution.py:77
  330.8 4.5 all-to-all-start.2
  335.9 20.1 %all-to-all-done.2 = bf16[8,384,256]{1,2,0:T(8,128)(2,1)S(1)} async-done(((bf16[8,384,256]{1,2,0:T(8,128)(2,1)}), bf16[8,384,256]{1,2,0:T(8,128)(2,1)S(1)}, u32[]{:S(2)}, u32[]{:S(2)}) %all-to-all-start.2) | async-done | bytes 1572896 | tf_op jit(solution)/shard_map/all_to_all | solution.py:13
  356.9 52.8 %all-gather.13.cloned.1.call-done = bf16[2048,512]{1,0:T(8,128)(2,1)} async-done(((bf16[64,512]{1,0:T(8,128)(2,1)}), bf16[2048,512]{1,0:T(8,128)(2,1)}) %all-gather.13.cloned.1.call-update) | async-done | bytes 2097168 | tf_op jit(solution)/shard_map/all_gather | solution.py:30
  409.7 1.8 convolution_convert_fusion.2
  411.6 1.5 collective-permute-start.1
  414.2 1.3 fusion.22
  443.3 1.6 pad.259
  446.4 1.7 pad.242
  448.8 41.6 %all-gather.5 = f32[32,2,256]{2,1,0:T(2,128)S(1)} all-gather(f32[1,2,256]{2,1,0:T(2,128)S(1)} %maximum_bitcast_fusion.1), channel_id=4, replica_groups=mesh['grp'=2,'sp'=32,'tp'=8] {'sp'}, dimensions={0}, use_global_device_ids=true | all-gather | bytes 67584 | tf_op jit(solution)/shard_map/all_gather | solution.py:48
  490.5 45.1 %all-gather.17.cloned.1.call-done = bf16[1,256,2048]{1,2,0:T(8,128)(2,1)} async-done(((bf16[1,256,64]{1,2,0:T(8,128)(2,1)}), bf16[1,256,2048]{1,2,0:T(8,128)(2,1)}) %all-gather.17.cloned.1.call-update) | async-done | bytes 1048592 | tf_op jit(solution)/shard_map/all_gather | solution.py:98
  535.7 3.9 convolution_convert_fusion
  539.7 46.7 %all_to_all.27 = bf16[8,384,256]{2,1,0:T(8,128)(2,1)S(1)} all-to-all(bf16[8,384,256]{2,1,0:T(8,128)(2,1)S(1)} %bitcast.109), channel_id=1, replica_groups=mesh['grp'=2,'sp'=32,'tp'=8] {'tp'}, dimensions={0} | all-to-all | bytes 3145728 | tf_op jit(solution)/shard_map/all_to_all | solution.py:77
  586.7 8.1 %all_to_all.28 = f32[8,1,384]{2,1,0:T(1,128)S(1)} all-to-all(f32[8,1,384]{2,1,0:T(1,128)S(1)} %broadcast_in_dim.8), channel_id=1, replica_groups=mesh['grp'=2,'sp'=32,'tp'=8] {'tp'}, dimensions={0} | all-to-all | bytes 24576 | tf_op jit(solution)/shard_map/all_to_all | solution.py:13
  (396 shorter events, 63.6 us)
Async XLA Ops:
  6.5 144.2 %all-gather.11.cloned.1.call-start = ((), (), s32[]{:S(2)}) async-start(), calls=%async_computation.5 | async-start | bytes 2162688 | tf_op jit(solution)/shard_map/all_gather | solution.py:30
  8.1 270.1 %all-gather.15.cloned.1.call-start = ((), (), s32[]{:S(2)}) async-start(), calls=%async_computation.7 | async-start | bytes 1081344 | tf_op jit(solution)/shard_map/all_gather | solution.py:98
  12.0 47.0 %copy-start.10 = (f32[2,2048]{1,0:T(2,128)S(1)}, f32[2,2048]{1,0:T(2,128)}, u32[]{:S(2)}) copy-start(f32[2,2048]{1,0:T(2,128)} %param.26) | copy-start | bytes 49156
  12.0 65.7 %all-to-all-start = ((bf16[8,384,256]{1,2,0:T(8,128)(2,1)}), bf16[8,384,256]{1,2,0:T(8,128)(2,1)S(1)}, u32[]{:S(2)}, u32[]{:S(2)}) async-start(bf16[8,384,256]{1,2,0:T(8,128)(2,1)} %broadcast_in_dim.6), calls=%async_computation | async-start | bytes 3145728 | tf_op jit(solution)/shard_map/all_to_all | solution.py:13
  57.1 352.6 %all-gather.13.cloned.1.call-start = ((), (), s32[]{:S(2)}) async-start(), calls=%async_computation.6 | async-start | bytes 2162688 | tf_op jit(solution)/shard_map/all_gather | solution.py:30
  78.6 76.7 %copy-start.31 = (f32[384,256]{1,0:T(8,128)S(1)}, f32[384,256]{1,0:T(8,128)}, u32[]{:S(2)}) copy-start(f32[384,256]{1,0:T(8,128)} %param.24) | copy-start | bytes 1179652
  78.6 76.7 %copy-start.33 = (bf16[2,1,256,256]{3,2,1,0:T(8,128)(2,1)S(1)}, bf16[2,1,256,256]{3,2,1,0:T(8,128)(2,1)}, u32[]{:S(2)}) copy-start(bf16[2,1,256,256]{3,2,1,0:T(8,128)(2,1)} %param.20) | copy-start | bytes 786436
  78.6 76.7 %copy-start.36 = (f32[384]{0:T(512)S(1)}, f32[384]{0:T(512)}, u32[]{:S(2)}) copy-start(f32[384]{0:T(512)} %param.23) | copy-start | bytes 4612
  152.7 2.5 collective-permute-start
  176.5 101.7 %copy-start.5 = (f32[384,256]{1,0:T(8,128)}, f32[384,256]{1,0:T(8,128)S(1)}, u32[]{:S(2)}) copy-start(f32[384,256]{1,0:T(8,128)S(1)} %pad.226) | copy-start | bytes 1179652
  177.2 101.0 %copy-start.6 = (f32[384,256]{1,0:T(8,128)}, f32[384,256]{1,0:T(8,128)S(1)}, u32[]{:S(2)}) copy-start(f32[384,256]{1,0:T(8,128)S(1)} %pad.211) | copy-start | bytes 1179652
  330.8 25.2 %all-to-all-start.2 = ((bf16[8,384,256]{1,2,0:T(8,128)(2,1)}), bf16[8,384,256]{1,2,0:T(8,128)(2,1)S(1)}, u32[]{:S(2)}, u32[]{:S(2)}) async-start(bf16[8,384,256]{1,2,0:T(8,128)(2,1)} %broadcast_in_dim.7), calls=%async_computation.2 | async-start | bytes 3145728 | tf_op jit(solution)/shard_map/all_to_all | solution.py:13
  335.3 200.3 %all-gather.17.cloned.1.call-start = ((), (), s32[]{:S(2)}) async-start(), calls=%async_computation.8 | async-start | bytes 1081344 | tf_op jit(solution)/shard_map/all_gather | solution.py:98
  356.8 56.7 %copy-start.12 = (f32[1,1,256]{2,1,0:T(1,128)S(1)}, f32[1,1,256]{2,1,0:T(1,128)}, u32[]{:S(2)}) copy-start(f32[1,1,256]{2,1,0:T(1,128)} %get-tuple-element.193) | copy-start | bytes 3076
  356.9 56.7 %copy-start.13 = (f32[1,1,256]{2,1,0:T(1,128)S(1)}, f32[1,1,256]{2,1,0:T(1,128)}, u32[]{:S(2)}) copy-start(f32[1,1,256]{2,1,0:T(1,128)} %get-tuple-element.194) | copy-start | bytes 3076
  356.9 56.7 %copy-start.14 = (f32[1,1,256]{2,1,0:T(1,128)S(1)}, f32[1,1,256]{2,1,0:T(1,128)}, u32[]{:S(2)}) copy-start(f32[1,1,256]{2,1,0:T(1,128)} %get-tuple-element.199) | copy-start | bytes 3076
  356.9 56.7 %copy-start.15 = (f32[1,1,256]{2,1,0:T(1,128)S(1)}, f32[1,1,256]{2,1,0:T(1,128)}, u32[]{:S(2)}) copy-start(f32[1,1,256]{2,1,0:T(1,128)} %get-tuple-element.200) | copy-start | bytes 3076
  356.9 56.9 %copy-start.30 = (f32[1,256]{1,0:T(1,128)S(1)}, f32[1,256]{1,0:T(1,128)}, u32[]{:S(2)}) copy-start(f32[1,256]{1,0:T(1,128)} %get-tuple-element.209) | copy-start | bytes 3076
  356.9 56.9 %copy-start.32 = (f32[384,256]{1,0:T(8,128)S(1)}, f32[384,256]{1,0:T(8,128)}, u32[]{:S(2)}) copy-start(f32[384,256]{1,0:T(8,128)} %param.24) | copy-start | bytes 1179652
  356.9 56.9 %copy-start.34 = (bf16[2,1,256,256]{3,2,1,0:T(8,128)(2,1)S(1)}, bf16[2,1,256,256]{3,2,1,0:T(8,128)(2,1)}, u32[]{:S(2)}) copy-start(bf16[2,1,256,256]{3,2,1,0:T(8,128)(2,1)} %param.20) | copy-start | bytes 786436
  356.9 56.9 %copy-start.37 = (f32[384]{0:T(512)S(1)}, f32[384]{0:T(512)}, u32[]{:S(2)}) copy-start(f32[384]{0:T(512)} %param.23) | copy-start | bytes 4612
  411.6 2.0 collective-permute-start.1
  445.6 90.0 %copy-start.3 = (f32[384,256]{1,0:T(8,128)}, f32[384,256]{1,0:T(8,128)S(1)}, u32[]{:S(2)}) copy-start(f32[384,256]{1,0:T(8,128)S(1)} %pad.258) | copy-start | bytes 1179652
  446.4 89.3 %copy-start.4 = (f32[384,256]{1,0:T(8,128)}, f32[384,256]{1,0:T(8,128)S(1)}, u32[]{:S(2)}) copy-start(f32[384,256]{1,0:T(8,128)S(1)} %pad.243) | copy-start | bytes 1179652
  (24 other events, 216.2 us)
Sparse Core Ops, SparseCore 0:
  9.4 141.3 all-gather.10
  152.9 125.2 all-gather.14
  280.3 129.3 all-gather.12
  411.6 123.9 all-gather.16
where the time goes:
time: 604 us; the launch traced here: 602 us
  waiting for transfers between devices  271 us (45%)
  blocking collectives  183 us (30%)
  starting transfers between devices  52.9 us (9%)
  local copies, waits for them, and re-layouts  42.2 us (7%)
  other arithmetic  24.4 us (4%)
  between operations  14.8 us (2%)
  matrix products  13.7 us (2%)
    all_gather x2, waiting for transfers between devices, in_one_piece(): whole = lax.all_gather(both, axis, axis=dim, tiled=True)  125 us
    all_gather x2, waiting for transfers between devices, fetch_layer(): lax.all_gather(exit_projector_matrix[tier_number], 'sp', axis=1, tiled=True)  105 us
    all_to_all x2, blocking collectives, summed_on_arrival(): lax.all_to_all(tiles, axis, split_axis=0, concat_axis=0, tiled=True)  92.9 us
    all_gather x2, blocking collectives, gathered_once(): both, at, found = (lax.all_gather(jnp.concatenate(lines), axis), 0, {})  82.5 us
    all_to_all x2, starting transfers between devices, sent_to_all(): return lax.all_to_all(copies, axis, split_axis=0, concat_axis=0, tiled=True)  49.6 us
    all_to_all x2, waiting for transfers between devices, sent_to_all(): return lax.all_to_all(copies, axis, split_axis=0, concat_axis=0, tiled=True)  38.8 us
    slice x114, local copies, waits for them, and re-layouts, on_device(): lax.associative_scan(combine_pairs, (keep_rate, driven), axis=0)  28.4 us
  transfers between devices with their start and end apart: 8, of which 8 were waited for; matrix products, arithmetic and copies ran while one was open for 12% of the time, Pallas kernels for 0%

commit v1 on v0

--- a/solution.py
+++ b/solution.py
@@ -2,6 +2,7 @@
 import jax.numpy as jnp
 from jax import lax
 from jax.sharding import PartitionSpec as P
+from jax.lax import all_gather
 
 BLOCK_W = 256
 EPSILON = 1e-06
@@ -92,10 +93,14 @@
 
 
 def fetch_layer(multiplier_matrix, memory_path_matrix, exit_projector_matrix, tier_number):
+
+    def treat_islands(row_axis, local_values):
+        return jnp.concatenate(all_gather(local_values, row_axis), 1)
+
     in_pair = in_one_piece(
         (multiplier_matrix[tier_number], memory_path_matrix[tier_number]), "sp", 0, 1
     )
-    out_full = lax.all_gather(exit_projector_matrix[tier_number], "sp", axis=1, tiled=True)
+    out_full = treat_islands("sp", local_values=exit_projector_matrix[tier_number])
     return (in_pair[0], in_pair[1], out_full)
 
 

time: 604 us -> 604 us (level)
  no operation moved by 1% of the time
where the time goes in v1:
time: 604 us; the launch traced here: 602 us
  waiting for transfers between devices  271 us (45%)
  blocking collectives  183 us (30%)
  starting transfers between devices  52.9 us (9%)
  local copies, waits for them, and re-layouts  42.2 us (7%)
  other arithmetic  24.4 us (4%)
  between operations  14.8 us (2%)
  matrix products  13.7 us (2%)
    all_gather x2, waiting for transfers between devices, in_one_piece(): whole = lax.all_gather(both, axis, axis=dim, tiled=True)  125 us
    all_gather x2, waiting for transfers between devices, treat_islands(): return jnp.concatenate(all_gather(local_values, row_axis), 1)  105 us
    all_to_all x2, blocking collectives, summed_on_arrival(): lax.all_to_all(tiles, axis, split_axis=0, concat_axis=0, tiled=True)  92.9 us
    all_gather x2, blocking collectives, gathered_once(): both, at, found = (lax.all_gather(jnp.concatenate(lines), axis), 0, {})  82.5 us
    all_to_all x2, starting transfers between devices, sent_to_all(): return lax.all_to_all(copies, axis, split_axis=0, concat_axis=0, tiled=True)  49.6 us
    all_to_all x2, waiting for transfers between devices, sent_to_all(): return lax.all_to_all(copies, axis, split_axis=0, concat_axis=0, tiled=True)  38.8 us
    slice x114, local copies, waits for them, and re-layouts, on_device(): lax.associative_scan(combine_pairs, (keep_rate, driven), axis=0)  28.4 us
  transfers between devices with their start and end apart: 8, of which 8 were waited for; matrix products, arithmetic and copies ran while one was open for 12% of the time, Pallas kernels for 0%

profile of v1, /device:TPU:33, one launch (start us, length us, event | category | flops | bytes accessed | tf_op | source)
XLA Modules:
  0.0 602.2 jit_solution(12787368369105031495)
XLA Ops:
  8.1 1.4 fusion.133
  12.0 45.1 %all-to-all-start = ((bf16[8,384,256]{1,2,0:T(8,128)(2,1)}), bf16[8,384,256]{1,2,0:T(8,128)(2,1)S(1)}, u32[]{:S(2)}, u32[]{:S(2)}) async-start(bf16[8,384,256]{1,2,0:T(8,128)(2,1)} %broadcast_in_dim.6), calls=%async_computation | async-start | bytes 3145728 | tf_op jit(solution)/shard_map/all_to_all | solution.py:14
  59.1 18.7 %all-to-all-done = bf16[8,384,256]{1,2,0:T(8,128)(2,1)S(1)} async-done(((bf16[8,384,256]{1,2,0:T(8,128)(2,1)}), bf16[8,384,256]{1,2,0:T(8,128)(2,1)S(1)}, u32[]{:S(2)}, u32[]{:S(2)}) %all-to-all-start) | async-done | bytes 1572896 | tf_op jit(solution)/shard_map/all_to_all | solution.py:14
  78.6 72.2 %all-gather.9.cloned.1.call-done = bf16[2048,512]{1,0:T(8,128)(2,1)} async-done(((bf16[64,512]{1,0:T(8,128)(2,1)}), bf16[2048,512]{1,0:T(8,128)(2,1)}) %all-gather.9.cloned.1.call-update) | async-done | bytes 2097168 | tf_op jit(solution)/shard_map/all_gather | solution.py:31
  150.8 1.8 convolution_convert_fusion.4
  152.7 1.7 collective-permute-start
  174.2 1.5 pad.227
  177.4 40.9 %all-gather.2 = f32[32,2,256]{2,1,0:T(2,128)S(1)} all-gather(f32[1,2,256]{2,1,0:T(2,128)S(1)} %maximum_bitcast_fusion), channel_id=2, replica_groups=mesh['grp'=2,'sp'=32,'tp'=8] {'sp'}, dimensions={0}, use_global_device_ids=true | all-gather | bytes 67584 | tf_op jit(solution)/shard_map/all_gather | solution.py:49
  218.4 59.8 %all-gather.11.cloned.1.call-done = bf16[32,256,64]{1,2,0:T(8,128)(2,1)} async-done(((bf16[1,256,64]{1,2,0:T(8,128)(2,1)}), bf16[32,256,64]{1,2,0:T(8,128)(2,1)}) %all-gather.11.cloned.1.call-update) | async-done | bytes 1048592 | tf_op jit(solution)/shard_map/all_gather | solution.py:98
  278.2 3.8 convolution_convert_fusion.1
  282.1 46.2 %all_to_all.26 = bf16[8,384,256]{2,1,0:T(8,128)(2,1)S(1)} all-to-all(bf16[8,384,256]{2,1,0:T(8,128)(2,1)S(1)} %bitcast.110), channel_id=1, replica_groups=mesh['grp'=2,'sp'=32,'tp'=8] {'tp'}, dimensions={0} | all-to-all | bytes 3145728 | tf_op jit(solution)/shard_map/all_to_all | solution.py:78
  330.8 4.5 all-to-all-start.2
  335.9 20.1 %all-to-all-done.2 = bf16[8,384,256]{1,2,0:T(8,128)(2,1)S(1)} async-done(((bf16[8,384,256]{1,2,0:T(8,128)(2,1)}), bf16[8,384,256]{1,2,0:T(8,128)(2,1)S(1)}, u32[]{:S(2)}, u32[]{:S(2)}) %all-to-all-start.2) | async-done | bytes 1572896 | tf_op jit(solution)/shard_map/all_to_all | solution.py:14
  356.9 52.8 %all-gather.13.cloned.1.call-done = bf16[2048,512]{1,0:T(8,128)(2,1)} async-done(((bf16[64,512]{1,0:T(8,128)(2,1)}), bf16[2048,512]{1,0:T(8,128)(2,1)}) %all-gather.13.cloned.1.call-update) | async-done | bytes 2097168 | tf_op jit(solution)/shard_map/all_gather | solution.py:31
  409.7 1.8 convolution_convert_fusion.2
  411.6 1.5 collective-permute-start.1
  414.2 1.3 fusion.22
  443.3 1.6 pad.259
  446.4 1.7 pad.242
  448.8 41.6 %all-gather.3 = f32[32,2,256]{2,1,0:T(2,128)S(1)} all-gather(f32[1,2,256]{2,1,0:T(2,128)S(1)} %maximum_bitcast_fusion.1), channel_id=3, replica_groups=mesh['grp'=2,'sp'=32,'tp'=8] {'sp'}, dimensions={0}, use_global_device_ids=true | all-gather | bytes 67584 | tf_op jit(solution)/shard_map/all_gather | solution.py:49
  490.5 45.1 %all-gather.15.cloned.1.call-done = bf16[32,256,64]{1,2,0:T(8,128)(2,1)} async-done(((bf16[1,256,64]{1,2,0:T(8,128)(2,1)}), bf16[32,256,64]{1,2,0:T(8,128)(2,1)}) %all-gather.15.cloned.1.call-update) | async-done | bytes 1048592 | tf_op jit(solution)/shard_map/all_gather | solution.py:98
  535.7 3.9 convolution_convert_fusion
  539.7 46.7 %all_to_all.27 = bf16[8,384,256]{2,1,0:T(8,128)(2,1)S(1)} all-to-all(bf16[8,384,256]{2,1,0:T(8,128)(2,1)S(1)} %bitcast.111), channel_id=1, replica_groups=mesh['grp'=2,'sp'=32,'tp'=8] {'tp'}, dimensions={0} | all-to-all | bytes 3145728 | tf_op jit(solution)/shard_map/all_to_all | solution.py:78
  586.7 8.1 %all_to_all.28 = f32[8,1,384]{2,1,0:T(1,128)S(1)} all-to-all(f32[8,1,384]{2,1,0:T(1,128)S(1)} %broadcast_in_dim.8), channel_id=1, replica_groups=mesh['grp'=2,'sp'=32,'tp'=8] {'tp'}, dimensions={0} | all-to-all | bytes 24576 | tf_op jit(solution)/shard_map/all_to_all | solution.py:14
  (396 shorter events, 63.6 us)
Async XLA Ops:
  6.5 144.2 %all-gather.9.cloned.1.call-start = ((), (), s32[]{:S(2)}) async-start(), calls=%async_computation.5 | async-start | bytes 2162688 | tf_op jit(solution)/shard_map/all_gather | solution.py:31
  8.1 270.1 %all-gather.11.cloned.1.call-start = ((), (), s32[]{:S(2)}) async-start(), calls=%async_computation.6 | async-start | bytes 1081344 | tf_op jit(solution)/shard_map/all_gather | solution.py:98
  12.0 47.0 %copy-start.10 = (f32[2,2048]{1,0:T(2,128)S(1)}, f32[2,2048]{1,0:T(2,128)}, u32[]{:S(2)}) copy-start(f32[2,2048]{1,0:T(2,128)} %param.26) | copy-start | bytes 49156
  12.0 65.7 %all-to-all-start = ((bf16[8,384,256]{1,2,0:T(8,128)(2,1)}), bf16[8,384,256]{1,2,0:T(8,128)(2,1)S(1)}, u32[]{:S(2)}, u32[]{:S(2)}) async-start(bf16[8,384,256]{1,2,0:T(8,128)(2,1)} %broadcast_in_dim.6), calls=%async_computation | async-start | bytes 3145728 | tf_op jit(solution)/shard_map/all_to_all | solution.py:14
  57.1 352.6 %all-gather.13.cloned.1.call-start = ((), (), s32[]{:S(2)}) async-start(), calls=%async_computation.7 | async-start | bytes 2162688 | tf_op jit(solution)/shard_map/all_gather | solution.py:31
  78.6 76.7 %copy-start.31 = (f32[384,256]{1,0:T(8,128)S(1)}, f32[384,256]{1,0:T(8,128)}, u32[]{:S(2)}) copy-start(f32[384,256]{1,0:T(8,128)} %param.24) | copy-start | bytes 1179652
  78.6 76.7 %copy-start.33 = (bf16[2,1,256,256]{3,2,1,0:T(8,128)(2,1)S(1)}, bf16[2,1,256,256]{3,2,1,0:T(8,128)(2,1)}, u32[]{:S(2)}) copy-start(bf16[2,1,256,256]{3,2,1,0:T(8,128)(2,1)} %param.20) | copy-start | bytes 786436
  78.6 76.7 %copy-start.36 = (f32[384]{0:T(512)S(1)}, f32[384]{0:T(512)}, u32[]{:S(2)}) copy-start(f32[384]{0:T(512)} %param.23) | copy-start | bytes 4612
  152.7 2.5 collective-permute-start
  176.5 101.7 %copy-start.5 = (f32[384,256]{1,0:T(8,128)}, f32[384,256]{1,0:T(8,128)S(1)}, u32[]{:S(2)}) copy-start(f32[384,256]{1,0:T(8,128)S(1)} %pad.226) | copy-start | bytes 1179652
  177.2 101.0 %copy-start.6 = (f32[384,256]{1,0:T(8,128)}, f32[384,256]{1,0:T(8,128)S(1)}, u32[]{:S(2)}) copy-start(f32[384,256]{1,0:T(8,128)S(1)} %pad.211) | copy-start | bytes 1179652
  330.8 25.2 %all-to-all-start.2 = ((bf16[8,384,256]{1,2,0:T(8,128)(2,1)}), bf16[8,384,256]{1,2,0:T(8,128)(2,1)S(1)}, u32[]{:S(2)}, u32[]{:S(2)}) async-start(bf16[8,384,256]{1,2,0:T(8,128)(2,1)} %broadcast_in_dim.7), calls=%async_computation.2 | async-start | bytes 3145728 | tf_op jit(solution)/shard_map/all_to_all | solution.py:14
  335.3 200.3 %all-gather.15.cloned.1.call-start = ((), (), s32[]{:S(2)}) async-start(), calls=%async_computation.8 | async-start | bytes 1081344 | tf_op jit(solution)/shard_map/all_gather | solution.py:98
  356.8 56.7 %copy-start.12 = (f32[1,1,256]{2,1,0:T(1,128)S(1)}, f32[1,1,256]{2,1,0:T(1,128)}, u32[]{:S(2)}) copy-start(f32[1,1,256]{2,1,0:T(1,128)} %get-tuple-element.193) | copy-start | bytes 3076
  356.9 56.7 %copy-start.13 = (f32[1,1,256]{2,1,0:T(1,128)S(1)}, f32[1,1,256]{2,1,0:T(1,128)}, u32[]{:S(2)}) copy-start(f32[1,1,256]{2,1,0:T(1,128)} %get-tuple-element.194) | copy-start | bytes 3076
  356.9 56.7 %copy-start.14 = (f32[1,1,256]{2,1,0:T(1,128)S(1)}, f32[1,1,256]{2,1,0:T(1,128)}, u32[]{:S(2)}) copy-start(f32[1,1,256]{2,1,0:T(1,128)} %get-tuple-element.199) | copy-start | bytes 3076
  356.9 56.7 %copy-start.15 = (f32[1,1,256]{2,1,0:T(1,128)S(1)}, f32[1,1,256]{2,1,0:T(1,128)}, u32[]{:S(2)}) copy-start(f32[1,1,256]{2,1,0:T(1,128)} %get-tuple-element.200) | copy-start | bytes 3076
  356.9 56.9 %copy-start.30 = (f32[1,256]{1,0:T(1,128)S(1)}, f32[1,256]{1,0:T(1,128)}, u32[]{:S(2)}) copy-start(f32[1,256]{1,0:T(1,128)} %get-tuple-element.209) | copy-start | bytes 3076
  356.9 56.9 %copy-start.32 = (f32[384,256]{1,0:T(8,128)S(1)}, f32[384,256]{1,0:T(8,128)}, u32[]{:S(2)}) copy-start(f32[384,256]{1,0:T(8,128)} %param.24) | copy-start | bytes 1179652
  356.9 56.9 %copy-start.34 = (bf16[2,1,256,256]{3,2,1,0:T(8,128)(2,1)S(1)}, bf16[2,1,256,256]{3,2,1,0:T(8,128)(2,1)}, u32[]{:S(2)}) copy-start(bf16[2,1,256,256]{3,2,1,0:T(8,128)(2,1)} %param.20) | copy-start | bytes 786436
  356.9 56.9 %copy-start.37 = (f32[384]{0:T(512)S(1)}, f32[384]{0:T(512)}, u32[]{:S(2)}) copy-start(f32[384]{0:T(512)} %param.23) | copy-start | bytes 4612
  411.6 2.0 collective-permute-start.1
  445.6 90.0 %copy-start.3 = (f32[384,256]{1,0:T(8,128)}, f32[384,256]{1,0:T(8,128)S(1)}, u32[]{:S(2)}) copy-start(f32[384,256]{1,0:T(8,128)S(1)} %pad.258) | copy-start | bytes 1179652
  446.4 89.3 %copy-start.4 = (f32[384,256]{1,0:T(8,128)}, f32[384,256]{1,0:T(8,128)S(1)}, u32[]{:S(2)}) copy-start(f32[384,256]{1,0:T(8,128)S(1)} %pad.243) | copy-start | bytes 1179652
  (24 other events, 216.2 us)
Sparse Core Ops, SparseCore 0:
  9.4 141.3 all-gather.8
  152.9 125.2 all-gather.10
  280.3 129.3 all-gather.12
  411.6 123.9 all-gather.14
